TPU v7x, 32 devices: a whole 2x2x4 slice. The times are simulated.
32 devices in a mesh: sp: 8 (over z, y), tp: 4 (over x, core).
Axes of the slice: x: 2, y: 2, z: 4, core: 2. Of those that a mesh axis runs over, the one named last changes fastest.
Arguments:
- inputs: bfloat16 [4096, 4096], P(('sp', 'tp')), may hold values from -42 to 42
- a_query_w: bfloat16 [4096, 2048], P(None, 'tp'), may hold values from -0.12570312 to 0.12570312
- a_key_w: bfloat16 [4096, 2048], P(None, 'tp'), may hold values from -0.12570312 to 0.12570312
- a_value_w: bfloat16 [4096, 2048], P(None, 'tp'), may hold values from -0.09375 to 0.09375
- b_query_w: bfloat16 [4096, 2048], P(None, 'tp'), may hold values from -0.12570312 to 0.12570312
- b_key_w: bfloat16 [4096, 512], P(None, 'tp'), may hold values from -0.12570312 to 0.12570312
- b_value_w: bfloat16 [4096, 512], P(None, 'tp'), may hold values from -0.09375 to 0.09375
- head_lambda: float32 [16], P('tp'), may hold values from 0.3 to 0.8
- head_gain: float32 [128], replicated, may hold values from 0.1 to 1.9
- sink_logit: float32 [32], P('tp'), may hold values from 2 to 7
- a_out_w: bfloat16 [2048, 4096], P('tp'), may hold values from -0.125 to 0.125
- b_out_w: bfloat16 [2048, 4096], P('tp'), may hold values from -0.625 to 0.625
Outputs:
- mixed: bfloat16 [4096, 4096], P(('sp', 'tp'))
All inputs are finite; a program needn't handle non-finite values.
Results may differ from a plain program's by a relative error of at most 0.015.
Values may be sent and summed in bfloat16 or wider, within the bound.
A program may use at most 128 MiB of HBM per device.

v0:
```python
import math

import jax
import jax.numpy as jnp
from jax import lax
from jax.sharding import PartitionSpec as P

HEAD_DIM = 64
VALUE_DIM = 128
WINDOW = 128


norm_eps = 0.0001
head_scale = 0.8
mask_fill = -1e30


def from_behind(value, axis, by):
    size = lax.axis_size(axis)
    pairs = [(i, i + by) for i in range(size) if 0 <= i + by < size]
    return lax.ppermute(value, axis, pairs)


def key_span(row_count):
    span_rows = math.gcd(row_count, 1024)
    return span_rows


def attend_block(carried, queries, query_pos, block_keys, block_values, key_pos):
    running, totals, numerator = carried
    scores = jnp.einsum(
        "qhmd,khmd->hmqk", queries, block_keys, preferred_element_type=jnp.float32
    ) * HEAD_DIM ** (-0.5)
    allowed = query_pos[:, None] >= key_pos[None, :]
    scores = jnp.where(allowed, scores, mask_fill)
    updated = jnp.maximum(running, jnp.max(scores, axis=-1))
    weights = jnp.where(allowed, jnp.exp(scores - updated[..., None]), 0.0)
    shrink = jnp.exp(running - updated)
    totals = totals * shrink + jnp.sum(weights, axis=-1)
    numerator = numerator * shrink[..., None] + jnp.einsum(
        "hmqk,khe->hmqe",
        weights.astype(jnp.bfloat16),
        block_values,
        preferred_element_type=jnp.float32,
    )
    return (updated, totals, numerator)


def advance(states, groups, key_rows, value_rows):
    row_count = key_rows.shape[0]
    span_rows = key_span(row_count)
    local_heads = value_rows.shape[1] // VALUE_DIM
    key_rows = key_rows.reshape(row_count, local_heads, 2, HEAD_DIM)
    value_rows = value_rows.reshape(row_count, local_heads, VALUE_DIM)

    def one_span(span_index, current):
        span_start = span_index * span_rows
        block_keys = lax.dynamic_slice_in_dim(key_rows, span_start, span_rows, 0)
        block_values = lax.dynamic_slice_in_dim(value_rows, span_start, span_rows, 0)
        key_pos = span_start + jnp.arange(span_rows, dtype=jnp.int32)
        results = []
        for query_group, carried in zip(groups, current):
            queries, query_pos = query_group

            def compute(given_state, queries=queries, query_pos=query_pos):
                return attend_block(
                    given_state, queries, query_pos, block_keys, block_values, key_pos
                )

            def unchanged(given_state):
                return given_state

            results.append(lax.cond(key_pos[0] <= query_pos[-1], compute, unchanged, carried))
        return tuple(results)

    return lax.fori_loop(0, row_count // span_rows, one_span, states)


def finish_heads(carried, head_lambda, head_gain):
    running, totals, numerator = carried
    means = numerator / totals[..., None]
    difference = means[:, 0] - head_lambda[:, None, None] * means[:, 1]
    mean_square = jnp.mean(difference * difference, axis=-1, keepdims=True)
    return (difference * lax.rsqrt(mean_square + norm_eps) * head_gain * head_scale).astype(
        jnp.bfloat16
    )


def shards(
    inputs,
    a_query_w,
    a_key_w,
    a_value_w,
    b_query_w,
    b_key_w,
    b_value_w,
    head_lambda,
    head_gain,
    sink_logit,
    a_out_w,
    b_out_w,
):
    matrices = (a_query_w, a_key_w, a_value_w, b_query_w, b_key_w, b_value_w)

    def project(shard_piece):
        return jnp.concatenate(
            [
                jnp.dot(shard_piece, matrix, preferred_element_type=jnp.float32).astype(
                    jnp.bfloat16
                )
                for matrix in matrices
            ],
            axis=1,
        )

    projected = project(lax.all_gather(inputs, "tp", axis=0, tiled=True))
    seg_rows = projected.shape[0]
    column_edges = [0]
    for matrix in matrices:
        column_edges.append(column_edges[-1] + matrix.shape[1])
    a_query = projected[:, column_edges[0] : column_edges[1]]
    a_key = projected[:, column_edges[1] : column_edges[2]]
    a_value = projected[:, column_edges[2] : column_edges[3]]
    b_query = projected[:, column_edges[3] : column_edges[4]]
    b_pair = projected[:, column_edges[4] : column_edges[6]]
    local_heads = head_lambda.shape[0]
    offset = lax.axis_index("sp") * seg_rows
    positions = offset + jnp.arange(seg_rows, dtype=jnp.int32)
    query_heads = a_query.reshape(seg_rows, local_heads, 2, HEAD_DIM)
    groups = ((query_heads, positions),)
    initial = tuple(
        (
            (
                jnp.full((local_heads, 2, group_queries.shape[0]), mask_fill, jnp.float32),
                jnp.zeros((local_heads, 2, group_queries.shape[0]), jnp.float32),
                jnp.zeros((local_heads, 2, group_queries.shape[0], VALUE_DIM), jnp.float32),
            )
            for group_queries, group_pos in groups
        )
    )
    earlier = from_behind(b_pair[seg_rows - WINDOW :], "sp", 1)
    shard_piece = (
        lax.all_gather(a_key, "sp", axis=0, tiled=True),
        lax.all_gather(a_value, "sp", axis=0, tiled=True),
    )
    states = advance(initial, groups, shard_piece[0], shard_piece[1])
    finished = [finish_heads(carried, head_lambda, head_gain) for carried in states]
    a_heads = finished[0]
    kv_heads = b_pair.shape[1] // (2 * HEAD_DIM)
    group_size = b_query.shape[1] // HEAD_DIM // kv_heads
    extended = jnp.concatenate([earlier, b_pair], axis=0)
    near_keys = extended[:, : kv_heads * HEAD_DIM].reshape(WINDOW + seg_rows, kv_heads, HEAD_DIM)
    near_values = extended[:, kv_heads * HEAD_DIM :].reshape(WINDOW + seg_rows, kv_heads, HEAD_DIM)
    window_queries = b_query.reshape(seg_rows, kv_heads, group_size, HEAD_DIM)
    sink_term = sink_logit.reshape(kv_heads, group_size)[:, :, None]
    query_span = math.gcd(seg_rows, 512)
    scores = jnp.einsum(
        "qhgd,khd->hgqk", window_queries, near_keys, preferred_element_type=jnp.float32
    ) * HEAD_DIM ** (-0.5)
    query_pos = offset + 0 + jnp.arange(query_span, dtype=jnp.int32)
    near_pos = offset + 0 - WINDOW + jnp.arange(query_span + WINDOW, dtype=jnp.int32)
    distance = query_pos[:, None] - near_pos[None, :]
    allowed = (distance >= 0) & (distance < WINDOW) & (near_pos[None, :] >= 0)
    scores = jnp.where(allowed, scores, mask_fill)
    row_top = jnp.maximum(jnp.max(scores, axis=-1), sink_term)
    weights = jnp.where(allowed, jnp.exp(scores - row_top[..., None]), 0.0)
    row_total = jnp.sum(weights, axis=-1) + jnp.exp(sink_term - row_top)
    probs = (weights / row_total[..., None]).astype(jnp.bfloat16)
    block_out = jnp.einsum("hgqk,khd->qhgd", probs, near_values, preferred_element_type=jnp.float32)
    outputs = block_out.astype(jnp.bfloat16).reshape(query_span, kv_heads * group_size * HEAD_DIM)
    a_weight = a_out_w.reshape(local_heads, VALUE_DIM, a_out_w.shape[1])
    return lax.psum_scatter(
        (
            jnp.einsum("hqe,hen->qn", a_heads, a_weight, preferred_element_type=jnp.float32)
            + jnp.dot(outputs, b_out_w, preferred_element_type=jnp.float32)
        ).astype(jnp.bfloat16),
        "tp",
        scatter_dimension=0,
        tiled=True,
    )


def solution(mesh):
    return jax.shard_map(
        shards,
        mesh=mesh,
        in_specs=(
            P(("sp", "tp"), None),
            P(None, "tp"),
            P(None, "tp"),
            P(None, "tp"),
            P(None, "tp"),
            P(None, "tp"),
            P(None, "tp"),
            P("tp"),
            P(),
            P("tp"),
            P("tp", None),
            P("tp", None),
        ),
        out_specs=P(("sp", "tp"), None),
        check_vma=False,
    )
```

profile of v0, /device:TPU:28, one launch (start us, length us, event | category | flops | bytes accessed | tf_op | source)
XLA Modules:
  0.0 340.4 jit_solution(8961619378976255206)
XLA Ops:
  7.3 37.0 %all-gather.4.cloned.1.call-done = bf16[512,4096]{1,0:T(8,128)(2,1)} async-done(((bf16[128,4096]{1,0:T(8,128)(2,1)}), bf16[512,4096]{1,0:T(8,128)(2,1)}) %all-gather.4.cloned.1.call-update) | async-done | bytes 4194320 | tf_op jit(solution)/shard_map/all_gather | solution.py:116
  44.3 6.6 %convolution_convert_fusion.1 = bf16[512,512]{1,0:T(8,128)(2,1)} fusion(bf16[512,4096]{1,0:T(8,128)(2,1)} %all-gather.4.cloned.1.call-done, bf16[4096,512]{1,0:T(8,128)(2,1)} %param.19), kind=kOutput, calls=%fused_computation.35 | convolution fusion | flops 2147745792 | bytes 8912896 | tf_op jit(solution)/shard_map/dot_general | solution.py:108
  51.5 6.6 %convolution_convert_fusion.3 = bf16[512,512]{1,0:T(8,128)(2,1)} fusion(bf16[512,4096]{1,0:T(8,128)(2,1)} %all-gather.4.cloned.1.call-done, bf16[4096,512]{1,0:T(8,128)(2,1)} %param.18), kind=kOutput, calls=%fused_computation.37 | convolution fusion | flops 2147745792 | bytes 8912896 | tf_op jit(solution)/shard_map/dot_general | solution.py:108
  58.2 4.1 %convolution_convert_fusion.4 = bf16[512,128]{0,1:T(8,128)(2,1)S(1)} fusion(bf16[512,4096]{1,0:T(8,128)(2,1)} %all-gather.4.cloned.1.call-done, bf16[4096,128]{1,0:T(8,128)(2,1)S(1)} %copy-done), kind=kOutput, calls=%fused_computation.39 | convolution fusion | flops 536936448 | bytes 5373952 | tf_op jit(solution)/shard_map/dot_general | solution.py:108
  65.7 2.4 convolution_convert_fusion
  68.1 3.2 convolution_convert_fusion.2
  73.2 2.5 fusion.19
  75.8 3.6 %fusion.23 = bf16[2,64,4,512]{3,1,2,0:T(8,128)(2,1)S(1)} fusion(bf16[640,2,64,1]{0,2,3,1:T(8,128)(2,1)S(1)} %bitcast.118, f32[2,640,512,4]{2,1,3,0:T(8,128)S(1)} %get-tuple-element.302, f32[2,4,512]{2,1,0:T(4,128)S(1)} %exponential_add_fusion, f32[2,4,512]{2,1,0:T(4,128)S(1)} %broadcast_maximum_fusion, pred[512,640]{0,1:T(8,128)(4,1)S(1)} %fusion.22), kind=kOutput, calls=%fused_computation.38 | convolution fusion | flops 351535104 | bytes 11534336 | tf_op jit(solution)/shard_map/hgqk,khd->qhgd/dot_general | solution.py:169
  79.5 5.7 %fusion.35 = f32[512,4096]{1,0:T(8,128)} fusion(bf16[512,512]{0,1:T(8,128)(2,1)S(1)} %bitcast.116, bf16[512,4096]{1,0:T(8,128)(2,1)S(1)} %copy-done.3), kind=kOutput, calls=%fused_computation.64 | convolution fusion | flops 2147483648 | bytes 13107200 | tf_op jit(solution)/shard_map/dot_general | solution.py:175
  85.1 37.8 %all-gather.8.cloned.1.call-done = bf16[4096,512]{1,0:T(8,128)(2,1)} async-done(((bf16[512,512]{1,0:T(8,128)(2,1)}), bf16[4096,512]{1,0:T(8,128)(2,1)}) %all-gather.8.cloned.1.call-update) | async-done | bytes 4194320 | tf_op jit(solution)/shard_map/all_gather | solution.py:144
  122.9 4.9 %copy_bitcast_fusion = bf16[4096,4,128]{2,0,1:T(8,128)(2,1)} fusion(bf16[4096,512]{1,0:T(8,128)(2,1)} %all-gather.8.cloned.1.call-done), kind=kLoop, calls=%fused_computation.29 | loop fusion | bytes 8388608 | tf_op jit(solution)/shard_map/while | solution.py:76
  127.8 68.6 %all-gather.6.cloned.1.call-done = bf16[4096,512]{1,0:T(8,128)(2,1)} async-done(((bf16[512,512]{1,0:T(8,128)(2,1)}), bf16[4096,512]{1,0:T(8,128)(2,1)}) %all-gather.6.cloned.1.call-update) | async-done | bytes 4194320 | tf_op jit(solution)/shard_map/all_gather | solution.py:143
  196.4 6.4 %copy.19 = bf16[4096,512]{0,1:T(8,128)(2,1)} copy(bf16[4096,512]{1,0:T(8,128)(2,1)} %all-gather.6.cloned.1.call-done) | data formatting | bytes 8388608 | tf_op jit(solution)/shard_map/all_gather | solution.py:143
  203.0 76.7 %while.17 = (s32[]{:T(128)}, f32[4,2,512]{2,1,0:T(2,128)S(1)}, f32[4,2,512]{2,1,0:T(2,128)S(1)}, f32[4,2,512,128]{3,2,1,0:T(8,128)S(1)}, s32[512]{0:T(512)S(1)},...) while((s32[]{:T(128)}, f32[4,2,512]{2,1,0:T(2,128)S(1)}, ...), condition=%wide.region_5.6_spmd, body=%wide.region_0.5_spmd.sunk | while | flops 1666720768 | bytes 59517248 | solution.py:76
  205.3 16.8 %conditional.2 = ((f32[4,2,512]{2,1,0:T(2,128)S(1)}, f32[4,2,512]{2,1,0:T(2,128)S(1)}, f32[4,2,512,128]{3,2,1,0:T(8,128)S(1)})) conditional(s32[]{:T(128)} %bitcast.106, (f32[4,2,512]{2,1,0:T(2,128)S(1)}, f32[4,2,512]{2,1,0:T(2,128)S(1)}, f32[4,2,512,128]{3,2,1,0:T(8,128)S(1)}) %tuple.53, (s32[512]{0:T(512)S(1)}, s32[1024]{0:T(1024)S(1)}, s32[]{:T(128)}, ...), branch_computations={%region_1.0_spmd, %region_2.4_spmd} | conditional | flops 1666719744 | bytes 59512908 | solution.py:73
  205.7 4.2 %fusion = (f32[4,2,512]{2,1,0:T(2,128)S(1)}, f32[4,2,1024,512]{3,2,1,0:T(8,128)S(1)}) fusion(pred[512,1024]{0,1:T(8,128)(4,1)S(1)} %broadcast_compare_fusion, bf16[512,4,2,64]{0,3,2,1:T(8,128)(2,1)} %get-tuple-element.243, bf16[4096,4,2,64]{0,3,2,1:T(8,128)(2,1)} %get-tuple-element.241, s32[]{:T(128)S(6)} %select_n.25), kind=kOutput, calls=%fused_computation.2 | convolution fusion | flops 549449728 | bytes 18890756 | tf_op jit(solution)/shard_map/while/body/eval_jaxpr/cond/branch_1_fun/qhmd,khmd->hmqk/dot_general | solution.py:31
  210.0 4.0 %fusion.2 = f32[4,2,512]{2,1,0:T(2,128)S(1)} fusion(f32[4,2,1024,512]{3,2,1,0:T(8,128)S(1)} %get-tuple-element.298, f32[4,2,512]{2,1,0:T(2,128)S(1)} %max.19, pred[512,1024]{0,1:T(8,128)(4,1)S(1)} %broadcast_compare_fusion), kind=kLoop, calls=%fused_computation.4 | loop fusion | flops 20967424 | bytes 17334272 | tf_op jit(solution)/shard_map/while/body/eval_jaxpr/cond/branch_1_fun/reduce_sum | solution.py:39
  214.0 8.1 %multiply_add_fusion = f32[4,2,512,128]{3,2,1,0:T(8,128)S(1)} fusion(f32[4,2,512,128]{3,2,1,0:T(8,128)S(1)} %get-tuple-element.245, f32[4,2,1024,512]{3,2,1,0:T(8,128)S(1)} %get-tuple-element.298, f32[4,2,512]{2,1,0:T(2,128)S(1)} %max.19, pred[512,1024]{0,1:T(8,128)(4,1)S(1)} %broadcast_compare_fusion, bf16[4096,4,128]{2,0,1:T(8,128)(2,1)} %get-tuple-element.246, ...), kind=kOutput, calls=%fused_computation.7 | convolution fusion | flops 1095761920 | bytes 22577156 | tf_op jit(solution)/shard_map/while/body/eval_jaxpr/cond/branch_1_fun/hmqk,khe->hmqe/dot_general | solution.py:40
  224.5 16.8 %conditional.2 = ((f32[4,2,512]{2,1,0:T(2,128)S(1)}, f32[4,2,512]{2,1,0:T(2,128)S(1)}, f32[4,2,512,128]{3,2,1,0:T(8,128)S(1)})) conditional(s32[]{:T(128)} %bitcast.106, (f32[4,2,512]{2,1,0:T(2,128)S(1)}, f32[4,2,512]{2,1,0:T(2,128)S(1)}, f32[4,2,512,128]{3,2,1,0:T(8,128)S(1)}) %tuple.53, (s32[512]{0:T(512)S(1)}, s32[1024]{0:T(1024)S(1)}, s32[]{:T(128)}, ...), branch_computations={%region_1.0_spmd, %region_2.4_spmd} | conditional | flops 1666719744 | bytes 59512908 | solution.py:73
  224.9 4.2 %fusion = (f32[4,2,512]{2,1,0:T(2,128)S(1)}, f32[4,2,1024,512]{3,2,1,0:T(8,128)S(1)}) fusion(pred[512,1024]{0,1:T(8,128)(4,1)S(1)} %broadcast_compare_fusion, bf16[512,4,2,64]{0,3,2,1:T(8,128)(2,1)} %get-tuple-element.243, bf16[4096,4,2,64]{0,3,2,1:T(8,128)(2,1)} %get-tuple-element.241, s32[]{:T(128)S(6)} %select_n.25), kind=kOutput, calls=%fused_computation.2 | convolution fusion | flops 549449728 | bytes 18890756 | tf_op jit(solution)/shard_map/while/body/eval_jaxpr/cond/branch_1_fun/qhmd,khmd->hmqk/dot_general | solution.py:31
  229.1 4.0 %fusion.2 = f32[4,2,512]{2,1,0:T(2,128)S(1)} fusion(f32[4,2,1024,512]{3,2,1,0:T(8,128)S(1)} %get-tuple-element.298, f32[4,2,512]{2,1,0:T(2,128)S(1)} %max.19, pred[512,1024]{0,1:T(8,128)(4,1)S(1)} %broadcast_compare_fusion), kind=kLoop, calls=%fused_computation.4 | loop fusion | flops 20967424 | bytes 17334272 | tf_op jit(solution)/shard_map/while/body/eval_jaxpr/cond/branch_1_fun/reduce_sum | solution.py:39
  233.2 8.1 %multiply_add_fusion = f32[4,2,512,128]{3,2,1,0:T(8,128)S(1)} fusion(f32[4,2,512,128]{3,2,1,0:T(8,128)S(1)} %get-tuple-element.245, f32[4,2,1024,512]{3,2,1,0:T(8,128)S(1)} %get-tuple-element.298, f32[4,2,512]{2,1,0:T(2,128)S(1)} %max.19, pred[512,1024]{0,1:T(8,128)(4,1)S(1)} %broadcast_compare_fusion, bf16[4096,4,128]{2,0,1:T(8,128)(2,1)} %get-tuple-element.246, ...), kind=kOutput, calls=%fused_computation.7 | convolution fusion | flops 1095761920 | bytes 22577156 | tf_op jit(solution)/shard_map/while/body/eval_jaxpr/cond/branch_1_fun/hmqk,khe->hmqe/dot_general | solution.py:40
  243.6 16.8 %conditional.2 = ((f32[4,2,512]{2,1,0:T(2,128)S(1)}, f32[4,2,512]{2,1,0:T(2,128)S(1)}, f32[4,2,512,128]{3,2,1,0:T(8,128)S(1)})) conditional(s32[]{:T(128)} %bitcast.106, (f32[4,2,512]{2,1,0:T(2,128)S(1)}, f32[4,2,512]{2,1,0:T(2,128)S(1)}, f32[4,2,512,128]{3,2,1,0:T(8,128)S(1)}) %tuple.53, (s32[512]{0:T(512)S(1)}, s32[1024]{0:T(1024)S(1)}, s32[]{:T(128)}, ...), branch_computations={%region_1.0_spmd, %region_2.4_spmd} | conditional | flops 1666719744 | bytes 59512908 | solution.py:73
  244.0 4.2 %fusion = (f32[4,2,512]{2,1,0:T(2,128)S(1)}, f32[4,2,1024,512]{3,2,1,0:T(8,128)S(1)}) fusion(pred[512,1024]{0,1:T(8,128)(4,1)S(1)} %broadcast_compare_fusion, bf16[512,4,2,64]{0,3,2,1:T(8,128)(2,1)} %get-tuple-element.243, bf16[4096,4,2,64]{0,3,2,1:T(8,128)(2,1)} %get-tuple-element.241, s32[]{:T(128)S(6)} %select_n.25), kind=kOutput, calls=%fused_computation.2 | convolution fusion | flops 549449728 | bytes 18890756 | tf_op jit(solution)/shard_map/while/body/eval_jaxpr/cond/branch_1_fun/qhmd,khmd->hmqk/dot_general | solution.py:31
  248.3 4.0 %fusion.2 = f32[4,2,512]{2,1,0:T(2,128)S(1)} fusion(f32[4,2,1024,512]{3,2,1,0:T(8,128)S(1)} %get-tuple-element.298, f32[4,2,512]{2,1,0:T(2,128)S(1)} %max.19, pred[512,1024]{0,1:T(8,128)(4,1)S(1)} %broadcast_compare_fusion), kind=kLoop, calls=%fused_computation.4 | loop fusion | flops 20967424 | bytes 17334272 | tf_op jit(solution)/shard_map/while/body/eval_jaxpr/cond/branch_1_fun/reduce_sum | solution.py:39
  252.4 8.1 %multiply_add_fusion = f32[4,2,512,128]{3,2,1,0:T(8,128)S(1)} fusion(f32[4,2,512,128]{3,2,1,0:T(8,128)S(1)} %get-tuple-element.245, f32[4,2,1024,512]{3,2,1,0:T(8,128)S(1)} %get-tuple-element.298, f32[4,2,512]{2,1,0:T(2,128)S(1)} %max.19, pred[512,1024]{0,1:T(8,128)(4,1)S(1)} %broadcast_compare_fusion, bf16[4096,4,128]{2,0,1:T(8,128)(2,1)} %get-tuple-element.246, ...), kind=kOutput, calls=%fused_computation.7 | convolution fusion | flops 1095761920 | bytes 22577156 | tf_op jit(solution)/shard_map/while/body/eval_jaxpr/cond/branch_1_fun/hmqk,khe->hmqe/dot_general | solution.py:40
  262.8 16.8 %conditional.2 = ((f32[4,2,512]{2,1,0:T(2,128)S(1)}, f32[4,2,512]{2,1,0:T(2,128)S(1)}, f32[4,2,512,128]{3,2,1,0:T(8,128)S(1)})) conditional(s32[]{:T(128)} %bitcast.106, (f32[4,2,512]{2,1,0:T(2,128)S(1)}, f32[4,2,512]{2,1,0:T(2,128)S(1)}, f32[4,2,512,128]{3,2,1,0:T(8,128)S(1)}) %tuple.53, (s32[512]{0:T(512)S(1)}, s32[1024]{0:T(1024)S(1)}, s32[]{:T(128)}, ...), branch_computations={%region_1.0_spmd, %region_2.4_spmd} | conditional | flops 1666719744 | bytes 59512908 | solution.py:73
  263.2 4.2 %fusion = (f32[4,2,512]{2,1,0:T(2,128)S(1)}, f32[4,2,1024,512]{3,2,1,0:T(8,128)S(1)}) fusion(pred[512,1024]{0,1:T(8,128)(4,1)S(1)} %broadcast_compare_fusion, bf16[512,4,2,64]{0,3,2,1:T(8,128)(2,1)} %get-tuple-element.243, bf16[4096,4,2,64]{0,3,2,1:T(8,128)(2,1)} %get-tuple-element.241, s32[]{:T(128)S(6)} %select_n.25), kind=kOutput, calls=%fused_computation.2 | convolution fusion | flops 549449728 | bytes 18890756 | tf_op jit(solution)/shard_map/while/body/eval_jaxpr/cond/branch_1_fun/qhmd,khmd->hmqk/dot_general | solution.py:31
  267.5 4.0 %fusion.2 = f32[4,2,512]{2,1,0:T(2,128)S(1)} fusion(f32[4,2,1024,512]{3,2,1,0:T(8,128)S(1)} %get-tuple-element.298, f32[4,2,512]{2,1,0:T(2,128)S(1)} %max.19, pred[512,1024]{0,1:T(8,128)(4,1)S(1)} %broadcast_compare_fusion), kind=kLoop, calls=%fused_computation.4 | loop fusion | flops 20967424 | bytes 17334272 | tf_op jit(solution)/shard_map/while/body/eval_jaxpr/cond/branch_1_fun/reduce_sum | solution.py:39
  271.5 8.1 %multiply_add_fusion = f32[4,2,512,128]{3,2,1,0:T(8,128)S(1)} fusion(f32[4,2,512,128]{3,2,1,0:T(8,128)S(1)} %get-tuple-element.245, f32[4,2,1024,512]{3,2,1,0:T(8,128)S(1)} %get-tuple-element.298, f32[4,2,512]{2,1,0:T(2,128)S(1)} %max.19, pred[512,1024]{0,1:T(8,128)(4,1)S(1)} %broadcast_compare_fusion, bf16[4096,4,128]{2,0,1:T(8,128)(2,1)} %get-tuple-element.246, ...), kind=kOutput, calls=%fused_computation.7 | convolution fusion | flops 1095761920 | bytes 22577156 | tf_op jit(solution)/shard_map/while/body/eval_jaxpr/cond/branch_1_fun/hmqk,khe->hmqe/dot_general | solution.py:40
  281.9 6.3 %fusion.18 = bf16[512,4096]{1,0:T(8,128)(2,1)} fusion(f32[512,4096]{1,0:T(8,128)} %fusion.35, bf16[4,128,4096]{2,1,0:T(8,128)(2,1)S(1)} %bitcast.108, f32[128]{0:T(128)S(1)} %copy-done.7, f32[4,512]{1,0:T(4,128)S(1)} %add_rsqrt_fusion, f32[4,2,512,128]{3,2,1,0:T(8,128)S(1)} %broadcast_divide_fusion, f32[4]{0:T(128)S(1)} %copy-done.6), kind=kOutput, calls=%fused_computation.26 | convolution fusion | flops 2153250816 | bytes 18883088 | tf_op jit(solution)/shard_map/hqe,hen->qn/dot_general | solution.py:174
  288.2 45.6 %reduce-scatter.2.cloned.1.call-done = bf16[128,4096]{1,0:T(8,128)(2,1)} async-done(((bf16[512,4096]{1,0:T(8,128)(2,1)}), bf16[128,4096]{1,0:T(8,128)(2,1)}) %reduce-scatter.2.cloned.1.call-update) | async-done | bytes 1048592 | tf_op jit(solution)/shard_map/reduce_scatter | solution.py:172
  (78 shorter events, 15.1 us)
Async XLA Ops:
  6.5 51.7 %copy-start = (bf16[4096,128]{1,0:T(8,128)(2,1)S(1)}, bf16[4096,128]{1,0:T(8,128)(2,1)}, u32[]{:S(2)}) copy-start(bf16[4096,128]{1,0:T(8,128)(2,1)} %param.22) | copy-start | bytes 3145732
  6.5 37.8 %all-gather.4.cloned.1.call-start = ((), (), s32[]{:S(2)}) async-start(), calls=%async_computation.1 | async-start | bytes 5242880 | tf_op jit(solution)/shard_map/all_gather | solution.py:116
  7.3 43.7 %copy-start.10 = (f32[8]{0:T(128)S(1)}, f32[8]{0:T(128)}, u32[]{:S(2)}) copy-start(f32[8]{0:T(128)} %param.25) | copy-start | bytes 100
  7.3 115.6 %all-gather.8.cloned.1.call-start = ((), (), s32[]{:S(2)}) async-start(), calls=%async_computation.3 | async-start | bytes 4718592 | tf_op jit(solution)/shard_map/all_gather | solution.py:144
  50.9 145.4 %all-gather.6.cloned.1.call-start = ((), (), s32[]{:S(2)}) async-start(), calls=%async_computation.2 | async-start | bytes 4718592 | tf_op jit(solution)/shard_map/all_gather | solution.py:143
  58.1 4.2 %copy-start.5 = (bf16[4096,128]{1,0:T(8,128)(2,1)S(1)}, bf16[4096,128]{1,0:T(8,128)(2,1)}, u32[]{:S(2)}) copy-start(bf16[4096,128]{1,0:T(8,128)(2,1)} %param.21) | copy-start | bytes 3145732
  58.2 275.7 %reduce-scatter.2.cloned.1.call-start = ((), (), s32[]{:S(2)}) async-start(), calls=%async_computation.4 | async-start | bytes 5242880 | tf_op jit(solution)/shard_map/reduce_scatter | solution.py:172
  58.2 4.1 %copy-start.2 = (bf16[512,4096]{1,0:T(8,128)(2,1)S(1)}, bf16[512,4096]{1,0:T(8,128)(2,1)}, u32[]{:S(2)}) copy-start(bf16[512,4096]{1,0:T(8,128)(2,1)} %all-gather.4.cloned.1.call-done) | copy-start | bytes 12582916
  62.3 3.3 copy-start.8
  63.9 4.1 %copy-start.9 = (bf16[4096,512]{1,0:T(8,128)(2,1)S(1)}, bf16[4096,512]{1,0:T(8,128)(2,1)}, u32[]{:S(2)}) copy-start(bf16[4096,512]{1,0:T(8,128)(2,1)} %param.17) | copy-start | bytes 12582916
  63.9 7.3 %collective-permute-start = (bf16[128,256]{0,1:T(8,128)(2,1)S(1)}, bf16[128,256]{0,1:T(8,128)(2,1)S(1)}, u32[]{:S(2)}, u32[]{:S(2)}) collective-permute-start(bf16[128,256]{0,1:T(8,128)(2,1)S(1)} %pad_maximum_fusion), channel_id=1, source_target_pairs={{0,4},{4,8},{8,12},{12,16},{16,20},{20,24},{24,28},{1,5},{5,9},{9,... | collective-permute-start | bytes 196616 | tf_op jit(solution)/shard_map/ppermute | solution.py:21
  75.8 3.7 %copy-start.3 = (bf16[512,4096]{1,0:T(8,128)(2,1)S(1)}, bf16[512,4096]{1,0:T(8,128)(2,1)}, u32[]{:S(2)}) copy-start(bf16[512,4096]{1,0:T(8,128)(2,1)} %param.27) | copy-start | bytes 12582916
  279.7 0.8 copy-start.6
  279.7 2.2 copy-start.4
  279.7 2.2 copy-start.7
  281.9 52.0 %copy-start.1 = (bf16[4096,128]{1,0:T(8,128)(2,1)S(1)}, bf16[4096,128]{1,0:T(8,128)(2,1)}, u32[]{:S(2)}) copy-start(bf16[4096,128]{1,0:T(8,128)(2,1)} %param.22) | copy-start | bytes 3145732
Sparse Core Ops, SparseCore 0:
  8.9 35.3 all-gather.3
  51.1 71.7 all-gather.7
  125.0 71.3 all-gather.5
  288.4 45.4 reduce-scatter.1
where the time goes:
time: 343 us; the launch traced here: 340 us
  waiting for transfers between devices  190 us (55%)
  matrix products  91.1 us (27%)
  other arithmetic  22.1 us (6%)
  local copies, waits for them, and re-layouts  17.1 us (5%)
  between operations  13.4 us (4%)
  loops' own time  5.19 us (2%)
    all_gather x1, waiting for transfers between devices, shards(): lax.all_gather(a_key, 'sp', axis=0, tiled=True)  68.6 us
    reduce_scatter x1, waiting for transfers between devices, shards(): lax.psum_scatter((jnp.einsum('hqe,hen->qn', a_heads, a_weight, preferred_...  45.6 us
    all_gather x1, waiting for transfers between devices, shards(): lax.all_gather(a_value, 'sp', axis=0, tiled=True)  37.8 us
    all_gather x1, waiting for transfers between devices, shards(): projected = project(lax.all_gather(inputs, 'tp', axis=0, tiled=True))  37 us
    dot_general x4, matrix products, attend_block(): jnp.einsum('hmqk,khe->hmqe', weights.astype(jnp.bfloat16), block_values,...  32.3 us
    dot_general x6, matrix products, project(): jnp.dot(shard_piece, matrix, preferred_element_type=jnp.float32)  24.4 us
    dot_general x4, matrix products, attend_block(): jnp.einsum('qhmd,khmd->hmqk', queries, block_keys, preferred_element_type...  16.9 us
    reduce_sum x4, other arithmetic, attend_block(): totals = totals * shrink + jnp.sum(weights, axis=-1)  16.2 us
  transfers between devices with their start and end apart: 5, of which 4 were waited for; matrix products, arithmetic and copies ran while one was open for 11% of the time, Pallas kernels for 0%

commit v1 on v0

v1 whole, which is shorter than its diff:
```python
import functools

import jax
import jax.numpy as jnp
from jax import lax
from jax.experimental import pallas as pl
from jax.experimental.pallas import tpu as pltpu
from jax.sharding import PartitionSpec as P

HEAD_DIM = 64
VALUE_DIM = 128
WINDOW = 128
norm_eps = 0.0001
head_scale = 0.8
mask_fill = -1e30
MESH = pl.DeviceIdType.MESH
F32 = jnp.float32
BF16 = jnp.bfloat16


def mm(a, b):
    return jnp.dot(a, b, preferred_element_type=F32)


def mm_t(a, b):
    return lax.dot_general(a, b, (((1,), (1,)), ((), ())), preferred_element_type=F32)


def attend_kernel(
    n, n_tp, n_split,
    lam, sink, aq, ak, av, bq, bk, bv, gain, wa_hbm, wb_hbm,
    out,
    kbuf, vbuf, qbuf, kext, vext, hbuf, obuf, qs, m_s, l_s, acc_s, b_heads,
    wa, wb, dsend, dbuf, own, xsend, xbuf,
    send_sem, recv_sem, ret_send, ret_recv, near_send, near_recv, w_sem,
    d_send, d_recv, x_send, x_recv,
):
    me = lax.axis_index("sp")
    t = lax.axis_index("tp")
    rows = aq.shape[0]
    sub = rows // n_split
    pair = jnp.where(lax.rem(t, 2) == 0, t + 1, t - 1)
    core = lax.rem(t, 2)
    chip = t // 2
    chips = n_tp // 2
    n_chunks = wa.shape[0]
    width = wa.shape[2]
    part = rows // n_tp

    barrier = pltpu.get_barrier_semaphore()
    for o in range(1, n):
        pl.semaphore_signal(barrier, inc=1, device_id={"sp": lax.rem(me + o, n)}, device_id_type=MESH)
    for o in range(1, n_tp):
        pl.semaphore_signal(barrier, inc=1, device_id={"tp": lax.rem(t + o, n_tp)}, device_id_type=MESH)
    pl.semaphore_wait(barrier, n - 1 + n_tp - 1)

    def subblock(source, j):
        return jnp.where(lax.rem(source, 2) == 0, j, n_split - 1 - j)

    def pieces(d):
        h = d // n_split
        start = pl.multiple_of(subblock(me, lax.rem(d, n_split)) * sub, sub)
        cols = pl.ds(pl.multiple_of(h * VALUE_DIM, VALUE_DIM), VALUE_DIM)
        return (
            (aq.at[pl.ds(start, sub), cols], qbuf),
            (ak.at[:, cols], kbuf),
            (av.at[:, cols], vbuf),
        )

    def near_copies():
        return [
            pltpu.make_async_remote_copy(
                src_ref=src.at[pl.ds(rows - WINDOW, WINDOW)],
                dst_ref=dst.at[pl.ds(0, WINDOW)],
                send_sem=near_send.at[c],
                recv_sem=near_recv.at[c],
                device_id={"sp": lax.rem(me + 1, n)},
                device_id_type=MESH,
            )
            for c, (src, dst) in enumerate(((bk, kext), (bv, vext)))
        ]

    @pl.when(me < n - 1)
    def _():
        for copy in near_copies():
            copy.start()

    def send_copies(o):
        d = lax.rem(me + o, n)
        return [
            pltpu.make_async_remote_copy(
                src_ref=src,
                dst_ref=dst.at[me],
                send_sem=send_sem.at[o, c],
                recv_sem=recv_sem.at[me, c],
                device_id={"sp": d},
                device_id_type=MESH,
            )
            for c, (src, dst) in enumerate(pieces(d))
        ]

    def local_copies():
        return [
            pltpu.make_async_copy(src, dst.at[me], recv_sem.at[me, c])
            for c, (src, dst) in enumerate(pieces(me))
        ]

    for copy in local_copies():
        copy.start()

    @pl.loop(1, n)
    def _(o):
        for copy in send_copies(o):
            copy.start()

    def weight_copies(cc):
        at = pl.ds(pl.multiple_of(cc * width, width), width)
        return (
            pltpu.make_async_copy(wa_hbm.at[:, at], wa.at[cc], w_sem.at[cc, 0]),
            pltpu.make_async_copy(wb_hbm.at[:, at], wb.at[cc], w_sem.at[cc, 1]),
        )

    @pl.loop(0, n_chunks)
    def _(cc):
        for copy in weight_copies(cc):
            copy.start()

    kext[pl.ds(WINDOW, rows)] = bk[...]
    vext[pl.ds(WINDOW, rows)] = bv[...]

    @pl.when(me == 0)
    def _():
        kext[pl.ds(0, WINDOW)] = jnp.zeros((WINDOW, kext.shape[1]), BF16)
        vext[pl.ds(0, WINDOW)] = jnp.zeros((WINDOW, vext.shape[1]), BF16)

    @pl.when(me > 0)
    def _():
        for copy in near_copies():
            copy.wait_recv()

    kv_heads = bk.shape[1] // HEAD_DIM
    group = bq.shape[1] // bk.shape[1]
    q_iota = lax.broadcasted_iota(jnp.int32, (WINDOW, 2 * WINDOW), 0)
    k_iota = lax.broadcasted_iota(jnp.int32, (WINDOW, 2 * WINDOW), 1)

    @pl.loop(0, rows // WINDOW)
    def _(b):
        base = pl.multiple_of(b * WINDOW, WINDOW)
        first = (b == 0) & (me == 0)
        distance = q_iota + WINDOW - k_iota
        low = jnp.where(first, WINDOW, 0)
        allowed = (distance >= 0) & (distance < WINDOW) & (k_iota >= low)
        queries = bq[pl.ds(base, WINDOW), :].astype(F32) * HEAD_DIM ** (-0.5)
        queries = queries.astype(BF16)
        keys = kext[pl.ds(base, 2 * WINDOW), :]
        values = vext[pl.ds(base, 2 * WINDOW), :]
        for g in range(kv_heads):
            key = keys[:, g * HEAD_DIM : (g + 1) * HEAD_DIM]
            value = values[:, g * HEAD_DIM : (g + 1) * HEAD_DIM]
            for two in range(group // 2):
                both = []
                for e in range(2):
                    h = g * group + two * 2 + e
                    s = mm_t(queries[:, h * HEAD_DIM : (h + 1) * HEAD_DIM], key)
                    s = jnp.where(allowed, s, mask_fill)
                    top = jnp.maximum(jnp.max(s, axis=-1, keepdims=True), sink[h])
                    p = jnp.exp(s - top)
                    total = jnp.sum(p, axis=-1, keepdims=True) + jnp.exp(sink[h] - top)
                    both.append(mm((p * (1.0 / total)).astype(BF16), value).astype(BF16))
                at = (g * group + two * 2) * HEAD_DIM
                b_heads[pl.ds(base, WINDOW), at : at + 2 * HEAD_DIM] = jnp.concatenate(both, axis=1)

    my_head = me // n_split
    my_part = lax.rem(me, n_split)
    lane = lax.broadcasted_iota(jnp.int32, (sub, VALUE_DIM), 1)

    def ret_copy(i):
        row = pl.ds(pl.multiple_of(subblock(i, my_part) * sub, sub), sub)
        return pltpu.make_async_remote_copy(
            src_ref=obuf.at[i],
            dst_ref=hbuf.at[my_head, row],
            send_sem=ret_send.at[i],
            recv_sem=ret_recv.at[me],
            device_id={"sp": i},
            device_id_type=MESH,
        )

    def ret_local(i):
        row = pl.ds(pl.multiple_of(subblock(i, my_part) * sub, sub), sub)
        return pltpu.make_async_copy(obuf.at[i], hbuf.at[my_head, row], ret_recv.at[me])

    @pl.loop(0, n)
    def _(i):
        for c, (buf) in enumerate((qbuf, kbuf, vbuf)):
            pltpu.make_async_copy(buf.at[i], buf.at[i], recv_sem.at[i, c]).wait()
        q = qbuf[i].astype(F32) * HEAD_DIM ** (-0.5)
        qs[0] = jnp.where(lane < HEAD_DIM, q, 0.0).astype(BF16)
        qs[1] = jnp.where(lane >= HEAD_DIM, q, 0.0).astype(BF16)
        m_s[...] = jnp.full(m_s.shape, mask_fill, F32)
        l_s[...] = jnp.zeros(l_s.shape, F32)
        acc_s[...] = jnp.zeros(acc_s.shape, F32)
        first_row = subblock(i, my_part) * sub

        def block(j, diagonal):
            k = kbuf[j]
            v = vbuf[j]
            for m in range(2):
                s = mm_t(qs[m], k)
                if diagonal:
                    qpos = first_row + lax.broadcasted_iota(jnp.int32, s.shape, 0)
                    s = jnp.where(lax.broadcasted_iota(jnp.int32, s.shape, 1) <= qpos, s, mask_fill)
                old = m_s[m]
                new = jnp.maximum(old, jnp.max(s, axis=-1, keepdims=True))
                shrink = jnp.exp(old - new)
                p = jnp.exp(s - new[:, :1])
                folded = p[:, :VALUE_DIM]
                for c in range(1, s.shape[1] // VALUE_DIM):
                    folded = folded + p[:, c * VALUE_DIM : (c + 1) * VALUE_DIM]
                m_s[m] = new
                l_s[m] = l_s[m] * shrink + folded
                acc_s[m] = acc_s[m] * shrink + mm(p.astype(BF16), v)

        @pl.loop(0, i)
        def _(j):
            block(j, False)

        block(i, True)
        mean = [acc_s[m] / jnp.sum(l_s[m], axis=-1, keepdims=True) for m in range(2)]
        diff = mean[0] - lam[my_head] * mean[1]
        square = jnp.mean(diff * diff, axis=-1, keepdims=True)
        obuf[i] = (diff * lax.rsqrt(square + norm_eps) * gain[...] * head_scale).astype(BF16)

        @pl.when(i == me)
        def _():
            ret_local(i).start()

        @pl.when(i != me)
        def _():
            ret_copy(i).start()

    @pl.loop(0, n)
    def _(d):
        row = pl.ds(pl.multiple_of(subblock(me, lax.rem(d, n_split)) * sub, sub), sub)
        place = hbuf.at[d // n_split, row]
        pltpu.make_async_copy(place, place, ret_recv.at[d]).wait()

    local_heads = hbuf.shape[0]

    def project(row, cc):
        total = mm(b_heads[pl.ds(row, part), :], wb[cc])
        for h in range(local_heads):
            total = total + mm(hbuf[h, pl.ds(row, part), :], wa[cc, h * VALUE_DIM : (h + 1) * VALUE_DIM, :])
        return total

    def row_of(x, c):
        return pl.multiple_of((2 * x + c) * part, part)

    def d_copy(cc):
        return pltpu.make_async_remote_copy(
            src_ref=dsend.at[cc], dst_ref=dbuf.at[cc],
            send_sem=d_send.at[cc], recv_sem=d_recv.at[cc],
            device_id={"tp": pair}, device_id_type=MESH,
        )

    def x_copy(cc, o):
        to = lax.rem(chip + o, chips)
        return pltpu.make_async_remote_copy(
            src_ref=xsend.at[cc, o - 1], dst_ref=xbuf.at[cc, o - 1],
            send_sem=x_send.at[cc, o - 1], recv_sem=x_recv.at[cc, o - 1],
            device_id={"tp": 2 * to + core}, device_id_type=MESH,
        )

    def pass_on(cc):
        d_copy(cc).wait_recv()
        for o in range(1, chips):
            xsend[cc, o - 1] = (own[cc, o] + dbuf[cc, o].astype(F32)).astype(BF16)
            x_copy(cc, o).start()

    @pl.loop(0, n_chunks)
    def _(cc):
        for copy in weight_copies(cc):
            copy.wait()
        for o in range(chips):
            dsend[cc, o] = project(row_of(lax.rem(chip + o, chips), 1 - core), cc).astype(BF16)
        d_copy(cc).start()
        for o in range(chips):
            own[cc, o] = project(row_of(lax.rem(chip + o, chips), core), cc)

        @pl.when(cc > 0)
        def _():
            pass_on(cc - 1)

    pass_on(n_chunks - 1)

    @pl.loop(0, n_chunks)
    def _(cc):
        total = own[cc, 0] + dbuf[cc, 0].astype(F32)
        for o in range(1, chips):
            x_copy(cc, o).wait_recv()
            total = total + xbuf[cc, o - 1].astype(F32)
        out[:, pl.ds(pl.multiple_of(cc * width, width), width)] = total.astype(BF16)

    @pl.when(me < n - 1)
    def _():
        for copy in near_copies():
            copy.wait_send()

    @pl.loop(1, n)
    def _(o):
        for copy in send_copies(o):
            copy.wait_send()

    @pl.loop(0, n)
    def _(i):
        @pl.when(i != me)
        def _():
            ret_copy(i).wait_send()

    @pl.loop(0, n_chunks)
    def _(cc):
        d_copy(cc).wait_send()
        for o in range(1, chips):
            x_copy(cc, o).wait_send()


def attend(n, n_tp, lam, sink, aq, ak, av, bq, bk, bv, gain, wa, wb):
    rows = aq.shape[0]
    local_heads = lam.shape[0]
    n_split = n // local_heads
    sub = rows // n_split
    model = wa.shape[1]
    width = 512
    n_chunks = model // width
    chips = n_tp // 2
    part = rows // n_tp
    vm = pl.BlockSpec(memory_space=pltpu.VMEM)
    sm = pl.BlockSpec(memory_space=pltpu.SMEM)
    hbm = pl.BlockSpec(memory_space=pl.ANY)
    dma = pltpu.SemaphoreType.DMA
    return pl.pallas_call(
        functools.partial(attend_kernel, n, n_tp, n_split),
        out_shape=jax.ShapeDtypeStruct((part, model), BF16),
        in_specs=[sm, sm, vm, vm, vm, vm, vm, vm, vm, hbm, hbm],
        out_specs=vm,
        scratch_shapes=[
            pltpu.VMEM((n, rows, VALUE_DIM), BF16),
            pltpu.VMEM((n, rows, VALUE_DIM), BF16),
            pltpu.VMEM((n, sub, VALUE_DIM), BF16),
            pltpu.VMEM((WINDOW + rows, bk.shape[1]), BF16),
            pltpu.VMEM((WINDOW + rows, bv.shape[1]), BF16),
            pltpu.VMEM((local_heads, rows, VALUE_DIM), BF16),
            pltpu.VMEM((n, sub, VALUE_DIM), BF16),
            pltpu.VMEM((2, sub, VALUE_DIM), BF16),
            pltpu.VMEM((2, sub, VALUE_DIM), F32),
            pltpu.VMEM((2, sub, VALUE_DIM), F32),
            pltpu.VMEM((2, sub, VALUE_DIM), F32),
            pltpu.VMEM(bq.shape, BF16),
            pltpu.VMEM((n_chunks, wa.shape[0], width), BF16),
            pltpu.VMEM((n_chunks, wb.shape[0], width), BF16),
            pltpu.VMEM((n_chunks, chips, part, width), BF16),
            pltpu.VMEM((n_chunks, chips, part, width), BF16),
            pltpu.VMEM((n_chunks, chips, part, width), F32),
            pltpu.VMEM((n_chunks, chips - 1, part, width), BF16),
            pltpu.VMEM((n_chunks, chips - 1, part, width), BF16),
            dma((n, 3)),
            dma((n, 3)),
            dma((n,)),
            dma((n,)),
            dma((2,)),
            dma((2,)),
            dma((n_chunks, 2)),
            dma((n_chunks,)),
            dma((n_chunks,)),
            dma((n_chunks, chips - 1)),
            dma((n_chunks, chips - 1)),
        ],
        compiler_params=pltpu.CompilerParams(
            collective_id=0, has_side_effects=True, vmem_limit_bytes=62 * 1024 * 1024
        ),
    )(lam, sink, aq, ak, av, bq, bk, bv, gain, wa, wb)


def solution(mesh):
    n, n_tp = mesh.shape["sp"], mesh.shape["tp"]

    def shards(
        inputs, a_query_w, a_key_w, a_value_w, b_query_w, b_key_w, b_value_w,
        head_lambda, head_gain, sink_logit, a_out_w, b_out_w,
    ):
        gathered = lax.all_gather(inputs, "tp", axis=0, tiled=True)
        projected = [
            mm(gathered, matrix).astype(BF16)
            for matrix in (a_query_w, a_key_w, a_value_w, b_query_w, b_key_w, b_value_w)
        ]
        return attend(
            n, n_tp, head_lambda, sink_logit, *projected, head_gain.reshape(1, VALUE_DIM), a_out_w, b_out_w
        )

    return jax.shard_map(
        shards,
        mesh=mesh,
        in_specs=(
            P(("sp", "tp"), None),
            P(None, "tp"),
            P(None, "tp"),
            P(None, "tp"),
            P(None, "tp"),
            P(None, "tp"),
            P(None, "tp"),
            P("tp"),
            P(),
            P("tp"),
            P("tp", None),
            P("tp", None),
        ),
        out_specs=P(("sp", "tp"), None),
        check_vma=False,
    )
```

time: 343 us -> 205 us (0.60)
  waiting for transfers between devices: 190 us -> 37.8 us
  Pallas kernels: 0 us -> 131 us
  matrix products: 91.1 us -> 20.8 us
  other arithmetic: 22.1 us -> 0 us
  local copies, waits for them, and re-layouts: 17.1 us -> 2.31 us
  loops' own time: 5.19 us -> 0 us
    pallas_call x0 -> x1, Pallas kernels: none -> 131 us  [attend(): pl.pallas_call(functools.partial(attend_kernel, n, n_tp, n_split), out_sh...]
    all_gather x3 -> x1, waiting for transfers between devices: 143 us -> 37.1 us  [shards(): gathered = lax.all_gather(inputs, 'tp', axis=0, tiled=True)]
    dot_general x18 -> x6, matrix products: 91.1 us -> 20.8 us  [mm(): return jnp.dot(a, b, preferred_element_type=F32)]
    reduce_scatter x1 -> x0, waiting for transfers between devices: 45.6 us -> none  [shards(): lax.psum_scatter((jnp.einsum('hqe,hen->qn', a_heads, a_weight, preferred_...]
    reduce_sum x6 -> x0, other arithmetic: 19.1 us -> none  [the longest x4 16.2 us: attend_block(): totals = totals * shrink + jnp.sum(weights, axis=-1)]
    all_gather x1 -> x0, local copies, waits for them, and re-layouts: 6.41 us -> none  [shards(): lax.all_gather(a_key, 'sp', axis=0, tiled=True)]
    another operation x5 -> x0, loops' own time: 5.19 us -> none  [the longest x1 4.9 us: advance(): return lax.fori_loop(0, row_count // span_rows, one_span, states)]
    while x1 -> x0, local copies, waits for them, and re-layouts: 4.87 us -> none  [advance(): return lax.fori_loop(0, row_count // span_rows, one_span, states)]
  transfers between devices with their start and end apart: 5 -> 1, of which waited for: 4 -> 1; matrix products, arithmetic and copies ran while one was open for 11% -> 0% of each run, Pallas kernels for 0% -> 0%
where the time goes in v1:
time: 205 us
  Pallas kernels  131 us (64%)
  waiting for transfers between devices  37.8 us (18%)
  matrix products  20.8 us (10%)
  between operations  13.4 us (7%)
  local copies, waits for them, and re-layouts  2.31 us (1%)
    pallas_call x1, Pallas kernels, attend(): pl.pallas_call(functools.partial(attend_kernel, n, n_tp, n_split), out_sh...  131 us
    all_gather x1, waiting for transfers between devices, shards(): gathered = lax.all_gather(inputs, 'tp', axis=0, tiled=True)  37.1 us
    dot_general x6, matrix products, mm(): return jnp.dot(a, b, preferred_element_type=F32)  20.8 us
  transfers between devices with their start and end apart: 1, of which 1 were waited for; matrix products, arithmetic and copies ran while one was open for 0% of the time, Pallas kernels for 0%

profile of v1, /device:TPU:28, one launch (start us, length us, event | category | flops | bytes accessed | tf_op | source)
XLA Modules:
  0.0 205.0 jit_solution(4860234782926357134)
XLA Ops:
  6.5 0.0 copy-start
  6.5 0.0 copy-start.6
  6.5 0.0 all-gather.2.cloned.1.call-start
  6.5 0.7 all-gather.2.cloned.1.call-update
  7.3 37.1 %all-gather.2.cloned.1.call-done = bf16[512,4096]{1,0:T(8,128)(2,1)} async-done(((bf16[128,4096]{1,0:T(8,128)(2,1)}), bf16[512,4096]{1,0:T(8,128)(2,1)}) %all-gather.2.cloned.1.call-update) | async-done | bytes 4194320 | tf_op jit(solution)/shard_map/all_gather | solution.py:390
  44.3 0.0 copy-done
  44.3 0.0 copy-start.1
  44.3 0.0 copy-start.5
  44.3 4.2 %convolution_convert_fusion.4.bv = bf16[512,128]{1,0:T(8,128)(2,1)} fusion(bf16[512,4096]{1,0:T(8,128)(2,1)} %all-gather.2.cloned.1.call-done, bf16[4096,128]{1,0:T(8,128)(2,1)S(1)} %copy-done), kind=kOutput, calls=%fused_computation.4 | convolution fusion | flops 536936448 | bytes 5373952 | tf_op jit(solution)/shard_map/dot_general | solution.py:22
  48.6 0.0 copy-done.6
  48.6 4.1 %convolution_convert_fusion.5.bk = bf16[512,128]{1,0:T(8,128)(2,1)} fusion(bf16[512,4096]{1,0:T(8,128)(2,1)} %all-gather.2.cloned.1.call-done, bf16[4096,128]{1,0:T(8,128)(2,1)S(1)} %copy-done.6), kind=kOutput, calls=%fused_computation.5 | convolution fusion | flops 536936448 | bytes 5373952 | tf_op jit(solution)/shard_map/dot_general | solution.py:22
  52.6 0.0 copy-done.1
  52.6 0.0 copy-done.5
  52.6 0.0 copy-start.2
  52.6 3.1 %convolution_convert_fusion.bq = bf16[512,512]{1,0:T(8,128)(2,1)} fusion(bf16[512,4096]{1,0:T(8,128)(2,1)S(1)} %copy-done.5, bf16[4096,512]{1,0:T(8,128)(2,1)S(1)} %copy-done.1), kind=kOutput, calls=%fused_computation | convolution fusion | flops 2147745792 | bytes 8912896 | tf_op jit(solution)/shard_map/dot_general | solution.py:22
  55.8 0.0 copy-done.2
  55.8 0.0 copy-start.3
  55.8 3.1 %convolution_convert_fusion.1.av = bf16[512,512]{1,0:T(8,128)(2,1)} fusion(bf16[512,4096]{1,0:T(8,128)(2,1)S(1)} %copy-done.5, bf16[4096,512]{1,0:T(8,128)(2,1)S(1)} %copy-done.2), kind=kOutput, calls=%fused_computation.1 | convolution fusion | flops 2147745792 | bytes 8912896 | tf_op jit(solution)/shard_map/dot_general | solution.py:22
  58.9 0.0 copy-done.3
  58.9 0.0 copy-start.4
  58.9 3.1 %convolution_convert_fusion.2.ak = bf16[512,512]{1,0:T(8,128)(2,1)} fusion(bf16[512,4096]{1,0:T(8,128)(2,1)S(1)} %copy-done.5, bf16[4096,512]{1,0:T(8,128)(2,1)S(1)} %copy-done.3), kind=kOutput, calls=%fused_computation.2 | convolution fusion | flops 2147745792 | bytes 8912896 | tf_op jit(solution)/shard_map/dot_general | solution.py:22
  62.1 0.0 copy-done.4
  62.1 3.1 %convolution_convert_fusion.3.aq = bf16[512,512]{1,0:T(8,128)(2,1)} fusion(bf16[512,4096]{1,0:T(8,128)(2,1)S(1)} %copy-done.5, bf16[4096,512]{1,0:T(8,128)(2,1)S(1)} %copy-done.4), kind=kOutput, calls=%fused_computation.3 | convolution fusion | flops 2147745792 | bytes 8912896 | tf_op jit(solution)/shard_map/dot_general | solution.py:22
  65.2 130.6 %shard_map.118 = bf16[128,4096]{1,0:T(8,128)(2,1)} custom-call(f32[4]{0:T(128)} %lam.1, f32[8]{0:T(128)} %sink.1, bf16[512,512]{1,0:T(8,128)(2,1)} %convolution_convert_fusion.3.aq, bf16[512,512]{1,0:T(8,128)(2,1)} %convolution_convert_fusion.2.ak, bf16[512,512]{1,0:T(8,128)(2,1)} %convolution_convert_fusion.1.av, ...), custom_call_target="tpu_custom_call" | custom-call | tf_op jit(solution)/shard_map/pallas_call | solution.py:340
  195.8 2.3 %copy.14 = bf16[128,4096]{1,0:T(8,128)(2,1)} copy(bf16[128,4096]{1,0:T(8,128)(2,1)} %shard_map.118) | data formatting | bytes 2097152
Async XLA Ops:
  6.5 37.8 %copy-start = (bf16[4096,128]{1,0:T(8,128)(2,1)S(1)}, bf16[4096,128]{1,0:T(8,128)(2,1)}, u32[]{:S(2)}) copy-start(bf16[4096,128]{1,0:T(8,128)(2,1)} %param.18) | copy-start | bytes 3145732
  6.5 42.0 %copy-start.6 = (bf16[4096,128]{1,0:T(8,128)(2,1)S(1)}, bf16[4096,128]{1,0:T(8,128)(2,1)}, u32[]{:S(2)}) copy-start(bf16[4096,128]{1,0:T(8,128)(2,1)} %param.17) | copy-start | bytes 3145732
  6.5 37.8 %all-gather.2.cloned.1.call-start = ((), (), s32[]{:S(2)}) async-start(), calls=%async_computation | async-start | bytes 5242880 | tf_op jit(solution)/shard_map/all_gather | solution.py:390
  44.3 8.3 %copy-start.1 = (bf16[4096,512]{1,0:T(8,128)(2,1)S(1)}, bf16[4096,512]{1,0:T(8,128)(2,1)}, u32[]{:S(2)}) copy-start(bf16[4096,512]{1,0:T(8,128)(2,1)} %param.16) | copy-start | bytes 12582916
  44.3 8.3 %copy-start.5 = (bf16[512,4096]{1,0:T(8,128)(2,1)S(1)}, bf16[512,4096]{1,0:T(8,128)(2,1)}, u32[]{:S(2)}) copy-start(bf16[512,4096]{1,0:T(8,128)(2,1)} %all-gather.2.cloned.1.call-done) | copy-start | bytes 12582916
  52.6 3.1 %copy-start.2 = (bf16[4096,512]{1,0:T(8,128)(2,1)S(1)}, bf16[4096,512]{1,0:T(8,128)(2,1)}, u32[]{:S(2)}) copy-start(bf16[4096,512]{1,0:T(8,128)(2,1)} %param.15) | copy-start | bytes 12582916
  55.8 3.1 %copy-start.3 = (bf16[4096,512]{1,0:T(8,128)(2,1)S(1)}, bf16[4096,512]{1,0:T(8,128)(2,1)}, u32[]{:S(2)}) copy-start(bf16[4096,512]{1,0:T(8,128)(2,1)} %param.14) | copy-start | bytes 12582916
  58.9 3.2 %copy-start.4 = (bf16[4096,512]{1,0:T(8,128)(2,1)S(1)}, bf16[4096,512]{1,0:T(8,128)(2,1)}, u32[]{:S(2)}) copy-start(bf16[4096,512]{1,0:T(8,128)(2,1)} %param.13) | copy-start | bytes 12582916
Sparse Core Ops, SparseCore 0:
  8.9 35.3 all-gather.1

commit v2 on v1

--- a/solution.py
+++ b/solution.py
@@ -28,11 +28,13 @@
 
 def attend_kernel(
     n, n_tp, n_split,
-    lam, sink, aq, ak, av, bq, bk, bv, gain, wa_hbm, wb_hbm,
+    lam, sink, gain, x_hbm, wq_hbm, wk_hbm, wv_hbm, bwq_hbm, bwk_hbm, bwv_hbm, wa_hbm, wb_hbm,
     out,
-    kbuf, vbuf, qbuf, kext, vext, hbuf, obuf, qs, m_s, l_s, acc_s, b_heads,
+    xown, xrem, wq, wk, wv, bwq, bwk, bwv, aq, akv, bq,
+    kv, qbuf, kext, vext, hbuf, obuf, qs, m_s, l_s, acc_s, b_heads,
     wa, wb, dsend, dbuf, own, xsend, xbuf,
-    send_sem, recv_sem, ret_send, ret_recv, near_send, near_recv, w_sem,
+    x_sem, p_sem, g_send, g_recv, f_send, f_recv, own_send, own_recv,
+    kv_send, kv_recv, q_send, q_recv, ret_send, ret_recv, near_send, near_recv, w_sem,
     d_send, d_recv, x_send, x_recv,
 ):
     me = lax.axis_index("sp")
@@ -46,6 +48,15 @@
     n_chunks = wa.shape[0]
     width = wa.shape[2]
     part = rows // n_tp
+    half = part // 2
+    model = x_hbm.shape[1]
+
+    x_copy_in = pltpu.make_async_copy(x_hbm, xown.at[core], x_sem)
+    x_copy_in.start()
+    weights = ((wk_hbm, wk), (wv_hbm, wv), (wq_hbm, wq), (bwk_hbm, bwk), (bwv_hbm, bwv), (bwq_hbm, bwq))
+    p_copies = [pltpu.make_async_copy(src, dst, p_sem.at[c]) for c, (src, dst) in enumerate(weights)]
+    for copy in p_copies:
+        copy.start()
 
     barrier = pltpu.get_barrier_semaphore()
     for o in range(1, n):
@@ -53,98 +64,188 @@
     for o in range(1, n_tp):
         pl.semaphore_signal(barrier, inc=1, device_id={"tp": lax.rem(t + o, n_tp)}, device_id_type=MESH)
     pl.semaphore_wait(barrier, n - 1 + n_tp - 1)
+    x_copy_in.wait()
+
+    def g_copy(o, hf):
+        return pltpu.make_async_remote_copy(
+            src_ref=xown.at[core, pl.ds(hf * half, half)], dst_ref=xrem.at[o - 1, hf, core],
+            send_sem=g_send.at[o - 1, hf], recv_sem=g_recv.at[o - 1, hf],
+            device_id={"tp": 2 * lax.rem(chip + o, chips) + core}, device_id_type=MESH,
+        )
+
+    def f_copy(o, hf, c):
+        return pltpu.make_async_remote_copy(
+            src_ref=xrem.at[o - 1, hf, c], dst_ref=xrem.at[o - 1, hf, c],
+            send_sem=f_send.at[o - 1, hf], recv_sem=f_recv.at[o - 1, hf],
+            device_id={"tp": pair}, device_id_type=MESH,
+        )
+
+    def own_copy(c):
+        return pltpu.make_async_remote_copy(
+            src_ref=xown.at[c], dst_ref=xown.at[c], send_sem=own_send, recv_sem=own_recv,
+            device_id={"tp": pair}, device_id_type=MESH,
+        )
+
+    for hf in range(2):
+        for o in range(1, chips):
+            g_copy(o, hf).start()
+    own_copy(core).start()
+
+    def weight_copies(cc):
+        at = pl.ds(pl.multiple_of(cc * width, width), width)
+        return (
+            pltpu.make_async_copy(wa_hbm.at[:, at], wa.at[cc], w_sem.at[cc, 0]),
+            pltpu.make_async_copy(wb_hbm.at[:, at], wb.at[cc], w_sem.at[cc, 1]),
+        )
+
+    def column_steps(w):
+        step = min(w.shape[1], 256)
+        return [(at, step) for at in range(0, w.shape[1], step)]
+
+    def project_rows(load, put, first=None):
+        for c, (_, w) in enumerate(weights):
+            if first is not None:
+                @pl.when(first)
+                def _():
+                    p_copies[c].wait()
+            for at, step in column_steps(w):
+                put(c, at, step, mm(load(), w[:, at : at + step]).astype(BF16))
+
+    def put_rows(c, at, step, row, value):
+        count = value.shape[0]
+        if c == 2:
+            aq[pl.ds(row, count), at : at + step] = value
+        elif c == 3:
+            kext[pl.ds(row + WINDOW, count), at : at + step] = value
+        elif c == 4:
+            vext[pl.ds(row + WINDOW, count), at : at + step] = value
+        else:
+            bq[pl.ds(row, count), at : at + step] = value
 
     def subblock(source, j):
         return jnp.where(lax.rem(source, 2) == 0, j, n_split - 1 - j)
 
-    def pieces(d):
-        h = d // n_split
+    def head_columns(d):
+        return pl.ds(pl.multiple_of(d // n_split * VALUE_DIM, VALUE_DIM), VALUE_DIM)
+
+    def send_kv(x, hf):
+        for kind in range(2):
+            for o in range(n):
+                d = lax.rem(me + o, n)
+                if hf is None:
+                    src = akv.at[kind, x, :, :, :, head_columns(d)]
+                    dst = kv.at[me, kind, x]
+                else:
+                    src = akv.at[kind, x, :, hf, :, head_columns(d)]
+                    dst = kv.at[me, kind, x, :, hf]
+                if o == 0:
+                    pltpu.make_async_copy(src, dst, kv_recv.at[me]).start()
+                else:
+                    pltpu.make_async_remote_copy(
+                        src_ref=src, dst_ref=dst, send_sem=kv_send.at[o], recv_sem=kv_recv.at[me],
+                        device_id={"sp": d}, device_id_type=MESH,
+                    ).start()
+
+    def q_piece(d):
         start = pl.multiple_of(subblock(me, lax.rem(d, n_split)) * sub, sub)
-        cols = pl.ds(pl.multiple_of(h * VALUE_DIM, VALUE_DIM), VALUE_DIM)
-        return (
-            (aq.at[pl.ds(start, sub), cols], qbuf),
-            (ak.at[:, cols], kbuf),
-            (av.at[:, cols], vbuf),
+        return aq.at[pl.ds(start, sub), head_columns(d)]
+
+    def q_copy(o):
+        d = lax.rem(me + o, n)
+        return pltpu.make_async_remote_copy(
+            src_ref=q_piece(d), dst_ref=qbuf.at[me], send_sem=q_send.at[o], recv_sem=q_recv.at[me],
+            device_id={"sp": d}, device_id_type=MESH,
         )
 
     def near_copies():
         return [
             pltpu.make_async_remote_copy(
-                src_ref=src.at[pl.ds(rows - WINDOW, WINDOW)],
-                dst_ref=dst.at[pl.ds(0, WINDOW)],
+                src_ref=buf.at[pl.ds(rows, WINDOW)],
+                dst_ref=buf.at[pl.ds(0, WINDOW)],
                 send_sem=near_send.at[c],
                 recv_sem=near_recv.at[c],
                 device_id={"sp": lax.rem(me + 1, n)},
                 device_id_type=MESH,
             )
-            for c, (src, dst) in enumerate(((bk, kext), (bv, vext)))
+            for c, buf in enumerate((kext, vext))
         ]
 
-    @pl.when(me < n - 1)
-    def _():
-        for copy in near_copies():
-            copy.start()
-
-    def send_copies(o):
-        d = lax.rem(me + o, n)
-        return [
-            pltpu.make_async_remote_copy(
-                src_ref=src,
-                dst_ref=dst.at[me],
-                send_sem=send_sem.at[o, c],
-                recv_sem=recv_sem.at[me, c],
-                device_id={"sp": d},
-                device_id_type=MESH,
-            )
-            for c, (src, dst) in enumerate(pieces(d))
-        ]
-
-    def local_copies():
-        return [
-            pltpu.make_async_copy(src, dst.at[me], recv_sem.at[me, c])
-            for c, (src, dst) in enumerate(pieces(me))
-        ]
-
-    for copy in local_copies():
-        copy.start()
-
-    @pl.loop(1, n)
-    def _(o):
-        for copy in send_copies(o):
-            copy.start()
-
-    def weight_copies(cc):
-        at = pl.ds(pl.multiple_of(cc * width, width), width)
-        return (
-            pltpu.make_async_copy(wa_hbm.at[:, at], wa.at[cc], w_sem.at[cc, 0]),
-            pltpu.make_async_copy(wb_hbm.at[:, at], wb.at[cc], w_sem.at[cc, 1]),
-        )
+    @pl.loop(0, 2)
+    def _(step):
+        c_of = jnp.where(step == 0, core, 1 - core)
+        row = pl.multiple_of((2 * chip + c_of) * part, part)
+
+        @pl.when(step == 1)
+        def _():
+            own_copy(1 - core).wait_recv()
+
+        def put(c, at, w, value):
+            if c < 2:
+                akv[c, chip, c_of, :, :, at : at + w] = value.reshape(2, half, w)
+            else:
+                put_rows(c, at, w, row, value)
+
+        project_rows(lambda: xown[c_of], put, first=step == 0)
+
+    send_kv(chip, None)
+
+    for o in range(1, chips):
+        x = lax.rem(chip + chips - o, chips)
+
+        @pl.loop(0, 2)
+        def _(hf):
+            g_copy(o, hf).wait_recv()
+            f_copy(o, hf, core).start()
+            f_copy(o, hf, 1 - core).wait_recv()
+
+            def put(c, at, w, value):
+                value = value.reshape(2, half, w)
+                for k in range(2):
+                    if c < 2:
+                        akv[c, x, k, hf, :, at : at + w] = value[k]
+                    else:
+                        row = pl.multiple_of((2 * x + k) * part + hf * half, half)
+                        put_rows(c, at, w, row, value[k])
+
+            project_rows(lambda: xrem[o - 1, hf].reshape(part, model), put)
+
+            if o == chips - 1:
+                @pl.when((hf == 1) & (me < n - 1))
+                def _():
+                    for copy in near_copies():
+                        copy.start()
+
+            send_kv(x, hf)
+
+    pltpu.make_async_copy(q_piece(me), qbuf.at[me], q_recv.at[me]).start()
+    for o in range(1, n):
+        q_copy(o).start()
 
     @pl.loop(0, n_chunks)
     def _(cc):
         for copy in weight_copies(cc):
             copy.start()
 
-    kext[pl.ds(WINDOW, rows)] = bk[...]
-    vext[pl.ds(WINDOW, rows)] = bv[...]
-
     @pl.when(me == 0)
     def _():
         kext[pl.ds(0, WINDOW)] = jnp.zeros((WINDOW, kext.shape[1]), BF16)
         vext[pl.ds(0, WINDOW)] = jnp.zeros((WINDOW, vext.shape[1]), BF16)
 
-    @pl.when(me > 0)
-    def _():
-        for copy in near_copies():
-            copy.wait_recv()
-
-    kv_heads = bk.shape[1] // HEAD_DIM
-    group = bq.shape[1] // bk.shape[1]
+    kv_heads = kext.shape[1] // HEAD_DIM
+    group = bq.shape[1] // kext.shape[1]
+    blocks = rows // WINDOW
     q_iota = lax.broadcasted_iota(jnp.int32, (WINDOW, 2 * WINDOW), 0)
     k_iota = lax.broadcasted_iota(jnp.int32, (WINDOW, 2 * WINDOW), 1)
 
-    @pl.loop(0, rows // WINDOW)
-    def _(b):
+    @pl.loop(0, blocks)
+    def _(step):
+        b = lax.rem(step + 1, blocks)
+
+        @pl.when((b == 0) & (me > 0))
+        def _():
+            for copy in near_copies():
+                copy.wait_recv()
+
         base = pl.multiple_of(b * WINDOW, WINDOW)
         first = (b == 0) & (me == 0)
         distance = q_iota + WINDOW - k_iota
@@ -191,8 +292,8 @@
 
     @pl.loop(0, n)
     def _(i):
-        for c, (buf) in enumerate((qbuf, kbuf, vbuf)):
-            pltpu.make_async_copy(buf.at[i], buf.at[i], recv_sem.at[i, c]).wait()
+        pltpu.make_async_copy(kv.at[i], kv.at[i], kv_recv.at[i]).wait()
+        pltpu.make_async_copy(qbuf.at[i], qbuf.at[i], q_recv.at[i]).wait()
         q = qbuf[i].astype(F32) * HEAD_DIM ** (-0.5)
         qs[0] = jnp.where(lane < HEAD_DIM, q, 0.0).astype(BF16)
         qs[1] = jnp.where(lane >= HEAD_DIM, q, 0.0).astype(BF16)
@@ -202,8 +303,8 @@
         first_row = subblock(i, my_part) * sub
 
         def block(j, diagonal):
-            k = kbuf[j]
-            v = vbuf[j]
+            k = kv[j, 0].reshape(rows, VALUE_DIM)
+            v = kv[j, 1].reshape(rows, VALUE_DIM)
             for m in range(2):
                 s = mm_t(qs[m], k)
                 if diagonal:
@@ -307,8 +408,14 @@
 
     @pl.loop(1, n)
     def _(o):
-        for copy in send_copies(o):
-            copy.wait_send()
+        pltpu.make_async_copy(kv.at[0], kv.at[0], kv_send.at[o]).wait()
+        q_copy(o).wait_send()
+
+    own_copy(core).wait_send()
+    for o in range(1, chips):
+        for hf in range(2):
+            g_copy(o, hf).wait_send()
+            f_copy(o, hf, core).wait_send()
 
     @pl.loop(0, n)
     def _(i):
@@ -323,16 +430,16 @@
             x_copy(cc, o).wait_send()
 
 
-def attend(n, n_tp, lam, sink, aq, ak, av, bq, bk, bv, gain, wa, wb):
-    rows = aq.shape[0]
+def attend(n, n_tp, lam, sink, gain, inputs, wq, wk, wv, bwq, bwk, bwv, wa, wb):
+    part, model = inputs.shape
+    rows = part * n_tp
+    half = part // 2
     local_heads = lam.shape[0]
     n_split = n // local_heads
     sub = rows // n_split
-    model = wa.shape[1]
     width = 512
     n_chunks = model // width
     chips = n_tp // 2
-    part = rows // n_tp
     vm = pl.BlockSpec(memory_space=pltpu.VMEM)
     sm = pl.BlockSpec(memory_space=pltpu.SMEM)
     hbm = pl.BlockSpec(memory_space=pl.ANY)
@@ -340,21 +447,31 @@
     return pl.pallas_call(
         functools.partial(attend_kernel, n, n_tp, n_split),
         out_shape=jax.ShapeDtypeStruct((part, model), BF16),
-        in_specs=[sm, sm, vm, vm, vm, vm, vm, vm, vm, hbm, hbm],
+        in_specs=[sm, sm, vm] + [hbm] * 9,
         out_specs=vm,
         scratch_shapes=[
-            pltpu.VMEM((n, rows, VALUE_DIM), BF16),
-            pltpu.VMEM((n, rows, VALUE_DIM), BF16),
+            pltpu.VMEM((2, part, model), BF16),
+            pltpu.VMEM((chips - 1, 2, 2, half, model), BF16),
+            pltpu.VMEM(wq.shape, BF16),
+            pltpu.VMEM(wk.shape, BF16),
+            pltpu.VMEM(wv.shape, BF16),
+            pltpu.VMEM(bwq.shape, BF16),
+            pltpu.VMEM(bwk.shape, BF16),
+            pltpu.VMEM(bwv.shape, BF16),
+            pltpu.VMEM((rows, wq.shape[1]), BF16),
+            pltpu.VMEM((2, chips, 2, 2, half, wk.shape[1]), BF16),
+            pltpu.VMEM((rows, bwq.shape[1]), BF16),
+            pltpu.VMEM((n, 2, chips, 2, 2, half, VALUE_DIM), BF16),
             pltpu.VMEM((n, sub, VALUE_DIM), BF16),
-            pltpu.VMEM((WINDOW + rows, bk.shape[1]), BF16),
-            pltpu.VMEM((WINDOW + rows, bv.shape[1]), BF16),
+            pltpu.VMEM((WINDOW + rows, bwk.shape[1]), BF16),
+            pltpu.VMEM((WINDOW + rows, bwv.shape[1]), BF16),
             pltpu.VMEM((local_heads, rows, VALUE_DIM), BF16),
             pltpu.VMEM((n, sub, VALUE_DIM), BF16),
             pltpu.VMEM((2, sub, VALUE_DIM), BF16),
             pltpu.VMEM((2, sub, VALUE_DIM), F32),
             pltpu.VMEM((2, sub, VALUE_DIM), F32),
             pltpu.VMEM((2, sub, VALUE_DIM), F32),
-            pltpu.VMEM(bq.shape, BF16),
+            pltpu.VMEM((rows, bwq.shape[1]), BF16),
             pltpu.VMEM((n_chunks, wa.shape[0], width), BF16),
             pltpu.VMEM((n_chunks, wb.shape[0], width), BF16),
             pltpu.VMEM((n_chunks, chips, part, width), BF16),
@@ -362,8 +479,18 @@
             pltpu.VMEM((n_chunks, chips, part, width), F32),
             pltpu.VMEM((n_chunks, chips - 1, part, width), BF16),
             pltpu.VMEM((n_chunks, chips - 1, part, width), BF16),
-            dma((n, 3)),
-            dma((n, 3)),
+            dma,
+            dma((6,)),
+            dma((chips - 1, 2)),
+            dma((chips - 1, 2)),
+            dma((chips - 1, 2)),
+            dma((chips - 1, 2)),
+            dma,
+            dma,
+            dma((n,)),
+            dma((n,)),
+            dma((n,)),
+            dma((n,)),
             dma((n,)),
             dma((n,)),
             dma((2,)),
@@ -375,9 +502,9 @@
             dma((n_chunks, chips - 1)),
         ],
         compiler_params=pltpu.CompilerParams(
-            collective_id=0, has_side_effects=True, vmem_limit_bytes=62 * 1024 * 1024
+            collective_id=0, has_side_effects=True, vmem_limit_bytes=63 * 1024 * 1024
         ),
-    )(lam, sink, aq, ak, av, bq, bk, bv, gain, wa, wb)
+    )(lam, sink, gain, inputs, wq, wk, wv, bwq, bwk, bwv, wa, wb)
 
 
 def solution(mesh):
@@ -387,13 +514,9 @@
         inputs, a_query_w, a_key_w, a_value_w, b_query_w, b_key_w, b_value_w,
         head_lambda, head_gain, sink_logit, a_out_w, b_out_w,
     ):
-        gathered = lax.all_gather(inputs, "tp", axis=0, tiled=True)
-        projected = [
-            mm(gathered, matrix).astype(BF16)
-            for matrix in (a_query_w, a_key_w, a_value_w, b_query_w, b_key_w, b_value_w)
-        ]
         return attend(
-            n, n_tp, head_lambda, sink_logit, *projected, head_gain.reshape(1, VALUE_DIM), a_out_w, b_out_w
+            n, n_tp, head_lambda, sink_logit, head_gain.reshape(1, VALUE_DIM), inputs,
+            a_query_w, a_key_w, a_value_w, b_query_w, b_key_w, b_value_w, a_out_w, b_out_w,
         )
 
     return jax.shard_map(

time: 205 us -> 141 us (0.69)
  waiting for transfers between devices: 37.8 us -> 0 us
  matrix products: 20.8 us -> 0 us
  between operations: 13.4 us -> 0.01 us
  Pallas kernels: 131 us -> 138 us
    all_gather x1 -> x0, waiting for transfers between devices: 37.1 us -> none  [shards(): gathered = lax.all_gather(inputs, 'tp', axis=0, tiled=True)]
    dot_general x6 -> x0, matrix products: 20.8 us -> none  [mm(): return jnp.dot(a, b, preferred_element_type=F32)]
    pallas_call x1, Pallas kernels: 131 us -> 138 us  [attend(): pl.pallas_call(functools.partial(attend_kernel, n, n_tp, n_split), out_sh...]
  transfers between devices with their start and end apart: 1 -> 0, of which waited for: 1 -> 0; matrix products, arithmetic and copies ran while one was open for 0% -> 0% of each run, Pallas kernels for 0% -> 0%
where the time goes in v2:
time: 141 us; the launch traced here: 140 us
  Pallas kernels  138 us (98%)
  local copies, waits for them, and re-layouts  2.29 us (2%)
    pallas_call x1, Pallas kernels, attend(): pl.pallas_call(functools.partial(attend_kernel, n, n_tp, n_split), out_sh...  138 us

profile of v2, /device:TPU:28, one launch (start us, length us, event | category | flops | bytes accessed | tf_op | source)
XLA Modules:
  0.0 140.5 jit_solution(3489199935095973441)
XLA Ops:
  0.0 138.2 %shard_map.118 = bf16[128,4096]{1,0:T(8,128)(2,1)} custom-call(f32[4]{0:T(128)} %lam.1, f32[8]{0:T(128)} %sink.1, f32[1,128]{1,0:T(1,128)} %bitcast.1, bf16[128,4096]{1,0:T(8,128)(2,1)} %x_hbm.1, bf16[4096,512]{1,0:T(8,128)(2,1)} %wq_hbm.1, bf16[4096,512]{1,0:T(8,128)(2,1)} %wk_hbm.1, bf16[4096,512]{1,0:T(8,128)(2,1)} %wv_hbm.1, bf16[4096,512]{1,0:T(8,128)(2,1)} %bwq_hbm.1, ...), custom_call_target="tpu_custom_call" | custom-call | tf_op jit(solution)/shard_map/pallas_call | solution.py:447
  138.2 2.3 %copy.14 = bf16[128,4096]{1,0:T(8,128)(2,1)} copy(bf16[128,4096]{1,0:T(8,128)(2,1)} %shard_map.118) | data formatting | bytes 2097152

commit v3 on v2

--- a/solution.py
+++ b/solution.py
@@ -279,7 +279,7 @@
         row = pl.ds(pl.multiple_of(subblock(i, my_part) * sub, sub), sub)
         return pltpu.make_async_remote_copy(
             src_ref=obuf.at[i],
-            dst_ref=hbuf.at[my_head, row],
+            dst_ref=hbuf.at[row, head_columns(me)],
             send_sem=ret_send.at[i],
             recv_sem=ret_recv.at[me],
             device_id={"sp": i},
@@ -288,7 +288,7 @@
 
     def ret_local(i):
         row = pl.ds(pl.multiple_of(subblock(i, my_part) * sub, sub), sub)
-        return pltpu.make_async_copy(obuf.at[i], hbuf.at[my_head, row], ret_recv.at[me])
+        return pltpu.make_async_copy(obuf.at[i], hbuf.at[row, head_columns(me)], ret_recv.at[me])
 
     @pl.loop(0, n)
     def _(i):
@@ -305,8 +305,8 @@
         def block(j, diagonal):
             k = kv[j, 0].reshape(rows, VALUE_DIM)
             v = kv[j, 1].reshape(rows, VALUE_DIM)
-            for m in range(2):
-                s = mm_t(qs[m], k)
+            both = [mm_t(qs[m], k) for m in range(2)]
+            for m, s in enumerate(both):
                 if diagonal:
                     qpos = first_row + lax.broadcasted_iota(jnp.int32, s.shape, 0)
                     s = jnp.where(lax.broadcasted_iota(jnp.int32, s.shape, 1) <= qpos, s, mask_fill)
@@ -342,16 +342,11 @@
     @pl.loop(0, n)
     def _(d):
         row = pl.ds(pl.multiple_of(subblock(me, lax.rem(d, n_split)) * sub, sub), sub)
-        place = hbuf.at[d // n_split, row]
+        place = hbuf.at[row, head_columns(d)]
         pltpu.make_async_copy(place, place, ret_recv.at[d]).wait()
 
-    local_heads = hbuf.shape[0]
-
     def project(row, cc):
-        total = mm(b_heads[pl.ds(row, part), :], wb[cc])
-        for h in range(local_heads):
-            total = total + mm(hbuf[h, pl.ds(row, part), :], wa[cc, h * VALUE_DIM : (h + 1) * VALUE_DIM, :])
-        return total
+        return mm(b_heads[pl.ds(row, part), :], wb[cc]) + mm(hbuf[pl.ds(row, part), :], wa[cc])
 
     def row_of(x, c):
         return pl.multiple_of((2 * x + c) * part, part)
@@ -465,7 +460,7 @@
             pltpu.VMEM((n, sub, VALUE_DIM), BF16),
             pltpu.VMEM((WINDOW + rows, bwk.shape[1]), BF16),
             pltpu.VMEM((WINDOW + rows, bwv.shape[1]), BF16),
-            pltpu.VMEM((local_heads, rows, VALUE_DIM), BF16),
+            pltpu.VMEM((rows, local_heads * VALUE_DIM), BF16),
             pltpu.VMEM((n, sub, VALUE_DIM), BF16),
             pltpu.VMEM((2, sub, VALUE_DIM), BF16),
             pltpu.VMEM((2, sub, VALUE_DIM), F32),

time: 141 us -> 137 us (0.972)
  Pallas kernels: 138 us -> 134 us
    pallas_call x1, Pallas kernels: 138 us -> 134 us  [attend(): pl.pallas_call(functools.partial(attend_kernel, n, n_tp, n_split), out_sh...]
where the time goes in v3:
time: 137 us; the launch traced here: 136 us
  Pallas kernels  134 us (98%)
  local copies, waits for them, and re-layouts  2.29 us (2%)
    pallas_call x1, Pallas kernels, attend(): pl.pallas_call(functools.partial(attend_kernel, n, n_tp, n_split), out_sh...  134 us

profile of v3, /device:TPU:28, one launch (start us, length us, event | category | flops | bytes accessed | tf_op | source)
XLA Modules:
  0.0 136.4 jit_solution(4041434246777160420)
XLA Ops:
  0.0 134.1 %shard_map.118 = bf16[128,4096]{1,0:T(8,128)(2,1)} custom-call(f32[4]{0:T(128)} %lam.1, f32[8]{0:T(128)} %sink.1, f32[1,128]{1,0:T(1,128)} %bitcast.1, bf16[128,4096]{1,0:T(8,128)(2,1)} %x_hbm.1, bf16[4096,512]{1,0:T(8,128)(2,1)} %wq_hbm.1, bf16[4096,512]{1,0:T(8,128)(2,1)} %wk_hbm.1, bf16[4096,512]{1,0:T(8,128)(2,1)} %wv_hbm.1, bf16[4096,512]{1,0:T(8,128)(2,1)} %bwq_hbm.1, ...), custom_call_target="tpu_custom_call" | custom-call | tf_op jit(solution)/shard_map/pallas_call | solution.py:442
  134.1 2.3 %copy.14 = bf16[128,4096]{1,0:T(8,128)(2,1)} copy(bf16[128,4096]{1,0:T(8,128)(2,1)} %shard_map.118) | data formatting | bytes 2097152
